TPU v7x, 32 devices: a whole 2x2x4 slice. The times are simulated.
32 devices in a mesh: sp: 4 (over z), dp: 8 (over y, x, core).
Axes of the slice: x: 2, y: 2, z: 4, core: 2. Of those that a mesh axis runs over, the one named last changes fastest.
Arguments:
- cotangent: bfloat16 [8, 512, 2048], P('dp', 'sp'), may hold values from -6 to 6
- unit_pre: bfloat16 [8, 512, 2048], P('dp', None, 'sp'), may hold values from -6 to 6
- gate_pre: bfloat16 [8, 512, 2048], P('dp', None, 'sp'), may hold values from -15 to 15
- out_weight: bfloat16 [2048, 2048], P('dp', 'sp'), may hold values from -0.125 to 0.125
- mix_weight: bfloat16 [8, 128, 128], replicated, may hold values from -0.5 to 0.5
- mix_bias: bfloat16 [8, 128], replicated, may hold values from 0.099609375 to 1.8984375
- norm_gain: bfloat16 [2048], P('sp'), may hold values from 0.099609375 to 1.8984375
- norm_shift: bfloat16 [2048], P('sp'), may hold values from -3 to 3
Outputs:
- unit_grad: bfloat16 [8, 512, 2048], P('dp', None, 'sp')
- gate_grad: bfloat16 [8, 512, 2048], P('dp', None, 'sp')
- out_weight_grad: float32 [2048, 2048], P('dp', 'sp')
- mix_weight_grad: float32 [8, 128, 128], replicated
- mix_bias_grad: float32 [8, 128], replicated
- gain_grad: float32 [2048], P('sp')
- shift_grad: float32 [2048], P('sp')
All inputs are finite; a program needn't handle non-finite values.
Results may differ from a plain program's by a relative error of at most 0.015.
Values may be sent and summed in bfloat16 or wider, within the bound.
No kernel may reach another device: no remote copies, remote signals or barrier semaphores. Data moves between devices by JAX's collectives and lax.ppermute only.
A program may use at most 64 MiB of HBM per device.

v0:
```python
import math
import jax
import jax.numpy as jnp
from jax import lax
from jax.sharding import PartitionSpec as P

GW = 2048
GROUPS = 8
BLK = 128
epsilon = 1e-05
tanh_coef = math.sqrt(2.0 / math.pi)


def gelu_slope(values):
    inner = tanh_coef * (values + 0.044715 * values * values * values)
    hyper = jnp.tanh(inner)
    return 0.5 * (1.0 + hyper) + 0.5 * values * (1.0 - hyper * hyper) * tanh_coef * (
        1.0 + 3.0 * 0.044715 * values * values
    )


def local(cotangent, unit_pre, gate_pre, out_weight, mix_weight, mix_bias, norm_gain, norm_shift):
    seq_len = unit_pre.shape[1]
    channels = unit_pre.shape[2]
    group_dim = GW // GROUPS
    span_width = min(channels, group_dim)
    groups_here = channels // span_width
    blocks = seq_len // BLK
    group_start = lax.axis_index("sp") * channels // group_dim
    units = unit_pre[0].astype(jnp.float32)
    gates = gate_pre[0].astype(jnp.float32)
    unit_act = jax.nn.gelu(units)
    gate_act = jax.nn.gelu(gates)
    moments = lax.psum((jnp.sum(gate_act, axis=-1), jnp.sum(gate_act * gate_act, axis=-1)), "sp")
    mean_val = moments[0] / GW
    var_val = moments[1] / GW - mean_val * mean_val
    rstd_val = lax.rsqrt(var_val + epsilon)
    centred = (gate_act - mean_val[:, None]) * rstd_val[:, None]
    gain_vec = norm_gain.astype(jnp.float32)
    normed = (centred * gain_vec + norm_shift.astype(jnp.float32)).astype(jnp.bfloat16)
    causal = jnp.arange(BLK)[:, None] >= jnp.arange(BLK)[None, :]
    local_weight = lax.dynamic_slice_in_dim(mix_weight, group_start, groups_here, 0)
    masked = jnp.where(causal[None], local_weight, jnp.zeros_like(local_weight))
    local_bias = lax.dynamic_slice_in_dim(mix_bias, group_start, groups_here, 0).astype(jnp.float32)
    normed_blocks = normed.reshape(blocks, BLK, groups_here, span_width)
    mixed = jnp.einsum("gts,nsgd->ntgd", masked, normed_blocks, preferred_element_type=jnp.float32)
    mixed = (mixed + local_bias.T[None, :, :, None]).reshape(seq_len, channels)
    gated = (unit_act * mixed).astype(jnp.bfloat16)
    weight_whole = lax.all_gather(out_weight, "dp", axis=0, tiled=True)
    dy_rows = lax.all_gather(cotangent, "sp", axis=1, tiled=True)[0]
    product = jnp.dot(dy_rows, weight_whole, preferred_element_type=jnp.float32)
    weight_part = lax.dot_general(
        dy_rows, gated, (((0,), (0,)), ((), ())), preferred_element_type=jnp.float32
    )
    token_count = lax.axis_size("dp") * seq_len
    norm_scale = 1.0 / math.sqrt(token_count)
    mix_scale = 1.0 / math.sqrt(token_count // BLK * group_dim)
    out_grad = (
        lax.psum_scatter(
            weight_part.astype(jnp.bfloat16), "dp", scatter_dimension=0, tiled=True
        ).astype(jnp.float32)
        * norm_scale
    )
    unit_grad = (product * mixed * gelu_slope(units)).astype(jnp.bfloat16)
    mix_grad = product * unit_act
    mix_round = mix_grad.astype(jnp.bfloat16).reshape(blocks, BLK, groups_here, span_width)
    mix_term = jnp.einsum(
        "ntgd,nsgd->gts", mix_round, normed_blocks, preferred_element_type=jnp.float32
    )
    mix_term = jnp.where(causal[None], mix_term, jnp.float32(0.0))
    bias_term = jnp.sum(mix_grad.reshape(blocks, BLK, groups_here, span_width), axis=(0, 3)).T
    normed_grad = jnp.einsum(
        "gts,ntgd->nsgd", masked, mix_round, preferred_element_type=jnp.float32
    ).reshape(seq_len, channels)
    gain_term = jnp.sum(normed_grad * centred, axis=0)
    shift_term = jnp.sum(normed_grad, axis=0)
    scaled = normed_grad * gain_vec
    back_sums = lax.psum((jnp.sum(scaled, axis=-1), jnp.sum(scaled * centred, axis=-1)), "sp")
    first_m = back_sums[0] / GW
    second_m = back_sums[1] / GW
    gate_grad = (
        rstd_val[:, None]
        * (scaled - first_m[:, None] - centred * second_m[:, None])
        * gelu_slope(gates)
    ).astype(jnp.bfloat16)
    empty_weight = jnp.zeros((GROUPS, BLK, BLK), jnp.float32)
    empty_bias = jnp.zeros((GROUPS, BLK), jnp.float32)
    mix_local, bias_local, gain_total, shift_total = (
        lax.psum(mix_term.astype(jnp.bfloat16), "dp").astype(jnp.float32),
        lax.psum(bias_term.astype(jnp.bfloat16), "dp").astype(jnp.float32),
        lax.psum(gain_term.astype(jnp.bfloat16), "dp").astype(jnp.float32),
        lax.psum(shift_term.astype(jnp.bfloat16), "dp").astype(jnp.float32),
    )
    full_weight = lax.dynamic_update_slice_in_dim(empty_weight, mix_local, group_start, 0)
    full_bias = lax.dynamic_update_slice_in_dim(empty_bias, bias_local, group_start, 0)
    full_weight, full_bias = (
        lax.psum(full_weight.astype(jnp.bfloat16), "sp").astype(jnp.float32),
        lax.psum(full_bias.astype(jnp.bfloat16), "sp").astype(jnp.float32),
    )
    return (
        unit_grad[None],
        gate_grad[None],
        out_grad,
        full_weight * mix_scale,
        full_bias * mix_scale,
        gain_total * norm_scale,
        shift_total * norm_scale,
    )


def solution(mesh):
    in_specs = (
        P("dp", "sp", None),
        P("dp", None, "sp"),
        P("dp", None, "sp"),
        P("dp", "sp"),
        P(),
        P(),
        P("sp"),
        P("sp"),
    )
    out_specs = (
        P("dp", None, "sp"),
        P("dp", None, "sp"),
        P("dp", "sp"),
        P(),
        P(),
        P("sp"),
        P("sp"),
    )
    return jax.shard_map(local, mesh=mesh, in_specs=in_specs, out_specs=out_specs, check_vma=False)
```

profile of v0, /device:TPU:0, one launch (start us, length us, event | category | flops | bytes accessed | tf_op | source)
XLA Modules:
  0.0 237.9 jit_solution(5552104702866696244)
XLA Ops:
  8.7 1.7 reshape.181
  11.7 1.3 copy.78
  13.5 13.9 %all-reduce.1 = (f32[512]{0:T(512)S(1)}, f32[512]{0:T(512)S(1)}) all-reduce(f32[512]{0:T(512)S(1)} %get-tuple-element.40, f32[512]{0:T(512)S(1)} %get-tuple-element.39), channel_id=1, replica_groups=mesh['sp'=4,'dp'=8] {'sp'}, use_global_device_ids=true, to_apply=%region_3.4 | all-reduce | flops 1024 | bytes 8192 | tf_op jit(solution)/shard_map/psum | solution.py:34
  28.2 3.3 %fusion.43 = (bf16[4,128,2,256]{1,3,0,2:T(8,128)(2,1)}, f32[4,128,2,256]{1,3,0,2:T(8,128)}) fusion(f32[4,128,2,256]{1,3,0,2:T(8,128)} %copy.78, f32[128,2]{0,1:T(2,128)S(1)} %convert_bitcast_fusion.1, bf16[8,128,128]{2,1,0:T(8,128)(2,1)S(1)} %copy-done.7, s32[]{:T(128)S(6)} %select_n.20, pred[128,128]{1,0:T(8,128)(4,1)S(1)} %iota_compare_fusion, ...), kind=kOutput, calls=%fused_computation.64 | convolution fusion | flops 73433088 | bytes 3761156 | tf_op jit(solution)/shard_map/gts,nsgd->ntgd/dot_general | solution.py:46
  31.5 1.5 copy.71
  33.0 1.0 copy.87
  34.1 24.0 %all-gather.3.cloned.1.call-done = bf16[1,512,2048]{2,1,0:T(8,128)(2,1)} async-done(((bf16[1,128,2048]{2,1,0:T(8,128)(2,1)}), bf16[1,512,2048]{2,1,0:T(8,128)(2,1)}) %all-gather.3.cloned.1.call-update) | async-done | bytes 2097168 | tf_op jit(solution)/shard_map/all_gather | solution.py:50
  58.0 28.5 %all-gather.5.cloned.1.call-done = bf16[2048,512]{1,0:T(8,128)(2,1)} async-done(((bf16[256,512]{1,0:T(8,128)(2,1)}), bf16[2048,512]{1,0:T(8,128)(2,1)}) %all-gather.5.cloned.1.call-update) | async-done | bytes 2097168 | tf_op jit(solution)/shard_map/all_gather | solution.py:49
  86.6 5.6 %fusion.85 = (bf16[512,512]{1,0:T(8,128)(2,1)}, f32[512,512]{1,0:T(8,128)S(1)}, bf16[1,512,512]{2,1,0:T(8,128)(2,1)}) fusion(bf16[1,512,512]{2,1,0:T(8,128)(2,1)S(1)} %copy-done.2, f32[512,512]{1,0:T(8,128)} %bitcast.107, bf16[2048,512]{1,0:T(8,128)(2,1)} %all-gather.5.cloned.1.call-done, bf16[1,512,2048]{2,1,0:T(8,128)(2,1)} %all-gather.3.cloned.1.call-done), kind=kOutput, calls=%fused_computation.126 | convolution fusion | flops 1081868288 | bytes 7864320 | tf_op jit(solution)/shard_map/dot_general | solution.py:51
  92.2 1.2 reshape.178
  93.3 1.4 fusion.10
  94.8 1.4 copy.79
  97.1 51.0 %all-reduce.6.cloned.1.call-done = bf16[2,128,128]{2,1,0:T(8,128)(2,1)} async-done(((bf16[2,128,128]{2,1,0:T(8,128)(2,1)}), bf16[2,128,128]{2,1,0:T(8,128)(2,1)}) %all-reduce.6.cloned.1.call-update) | async-done | bytes 65552 | tf_op jit(solution)/shard_map/psum | solution.py:89
  149.7 4.3 %fusion = bf16[2048,512]{0,1:T(8,128)(2,1)} fusion(bf16[512,512]{1,0:T(8,128)(2,1)} %bitcast.108, bf16[1,512,2048]{2,1,0:T(8,128)(2,1)} %all-gather.3.cloned.1.call-done), kind=kOutput, calls=%fused_computation.13 | convolution fusion | flops 1074790400 | bytes 4718592 | tf_op jit(solution)/shard_map/dot_general | solution.py:52
  154.1 1.0 copy-done.4
  155.1 1.8 multiply_reduce_fusion
  158.1 1.6 copy.73
  160.5 11.8 %all-reduce.2 = (bf16[2,128]{1,0:T(2,128)(2,1)S(1)}, bf16[512]{0:T(512)(128)(2,1)S(1)}, bf16[512]{0:T(512)(128)(2,1)S(1)}) all-reduce(bf16[2,128]{1,0:T(2,128)(2,1)S(1)} %bitcast.114, bf16[512]{0:T(512)(128)(2,1)S(1)} %bitcast.112, bf16[512]{0:T(512)(128)(2,1)S(1)} %bitcast.113), channel_id=1, replica_groups=mesh['sp'=4,'dp'=8] {'dp'}, use_global_device_ids=true, to_apply=%region_12.13 | all-reduce | flops 1280 | bytes 5120 | tf_op jit(solution)/shard_map/psum | solution.py:90
  172.4 12.0 %psum.77 = bf16[8,128]{1,0:T(8,128)(2,1)S(1)} all-reduce(bf16[8,128]{1,0:T(8,128)(2,1)S(1)} %dynamic_update_slice.7), channel_id=1, replica_groups=mesh['sp'=4,'dp'=8] {'sp'}, use_global_device_ids=true, to_apply=%region_13.14 | all-reduce | flops 1024 | bytes 4096 | tf_op jit(solution)/shard_map/psum | solution.py:98
  184.4 8.4 %all-reduce = (f32[512]{0:T(512)S(1)}, f32[512]{0:T(512)S(1)}) all-reduce(f32[512]{0:T(512)S(1)} %bitcast.115, f32[512]{0:T(512)S(1)} %bitcast.116), channel_id=1, replica_groups=mesh['sp'=4,'dp'=8] {'sp'}, use_global_device_ids=true, to_apply=%region_7.8 | all-reduce | flops 1024 | bytes 8192 | tf_op jit(solution)/shard_map/psum | solution.py:78
  193.9 2.1 fusion.69
  196.1 1.8 convert_multiply_fusion.9
  197.9 31.5 %reduce-scatter.2.cloned.1.call-done = bf16[256,512]{0,1:T(8,128)(2,1)} async-done(((bf16[2048,512]{0,1:T(8,128)(2,1)}), bf16[256,512]{0,1:T(8,128)(2,1)}) %reduce-scatter.2.cloned.1.call-update) | async-done | bytes 262160 | tf_op jit(solution)/shard_map/reduce_scatter | solution.py:59
  230.4 1.0 copy.83
  (50 shorter events, 10.8 us)
Async XLA Ops:
  7.2 50.9 %all-gather.3.cloned.1.call-start = ((), (), s32[]{:S(2)}) async-start(), calls=%async_computation.1 | async-start | bytes 2621440 | tf_op jit(solution)/shard_map/all_gather | solution.py:50
  7.9 3.0 %copy-start.5 = (bf16[512]{0:T(512)(128)(2,1)S(1)}, bf16[512]{0:T(512)(128)(2,1)}, u32[]{:S(2)}) copy-start(bf16[512]{0:T(512)(128)(2,1)} %param.14) | copy-start | bytes 3076
  7.9 3.1 %copy-start.6 = (bf16[512]{0:T(512)(128)(2,1)S(1)}, bf16[512]{0:T(512)(128)(2,1)}, u32[]{:S(2)}) copy-start(bf16[512]{0:T(512)(128)(2,1)} %param.15) | copy-start | bytes 3076
  7.9 3.1 %copy-start.2 = (bf16[1,512,512]{2,1,0:T(8,128)(2,1)S(1)}, bf16[1,512,512]{2,1,0:T(8,128)(2,1)}, u32[]{:S(2)}) copy-start(bf16[1,512,512]{2,1,0:T(8,128)(2,1)} %param.9) | copy-start | bytes 1572868
  7.9 78.7 %all-gather.5.cloned.1.call-start = ((), (), s32[]{:S(2)}) async-start(), calls=%async_computation.2 | async-start | bytes 2359296 | tf_op jit(solution)/shard_map/all_gather | solution.py:49
  8.7 139.4 %all-reduce.6.cloned.1.call-start = ((), (), s32[]{:S(2)}) async-start(), calls=%async_computation.4 | async-start | bytes 131072 | tf_op jit(solution)/shard_map/psum | solution.py:89
  11.0 2.0 copy-start
  11.0 17.2 %copy-start.7 = (bf16[8,128,128]{2,1,0:T(8,128)(2,1)S(1)}, bf16[8,128,128]{2,1,0:T(8,128)(2,1)}, u32[]{:S(2)}) copy-start(bf16[8,128,128]{2,1,0:T(8,128)(2,1)} %param.12) | copy-start | bytes 786436
  93.3 1.4 copy-start.3
  94.7 101.3 %all-reduce.8.cloned.1.call-start = ((), (), s32[]{:S(2)}) async-start(), calls=%async_computation.5 | async-start | bytes 524288 | tf_op jit(solution)/shard_map/psum | solution.py:97
  149.0 0.7 copy-start.1
  149.7 79.7 %reduce-scatter.2.cloned.1.call-start = ((), (), s32[]{:S(2)}) async-start(), calls=%async_computation.3 | async-start | bytes 2359296 | tf_op jit(solution)/shard_map/reduce_scatter | solution.py:59
  154.1 1.1 copy-start.4
Sparse Core Ops, SparseCore 0:
  9.5 48.4 all-gather.2
  59.9 26.6 all-gather.4
  94.9 53.1 all-reduce.5
  150.3 35.0 all-reduce.7
  188.4 40.9 reduce-scatter.1
where the time goes:
time: 238 us
  waiting for transfers between devices  136 us (57%)
  blocking collectives  46.1 us (19%)
  matrix products  16.3 us (7%)
  local copies, waits for them, and re-layouts  16.2 us (7%)
  between operations  14 us (6%)
  other arithmetic  8.61 us (4%)
    psum x1, waiting for transfers between devices, local(): lax.psum(mix_term.astype(jnp.bfloat16), 'dp').astype(jnp.float32)  51 us
    reduce_scatter x1, waiting for transfers between devices, local(): lax.psum_scatter(weight_part.astype(jnp.bfloat16), 'dp', scatter_dimensio...  31.5 us
    all_gather x1, waiting for transfers between devices, local(): weight_whole = lax.all_gather(out_weight, 'dp', axis=0, tiled=True)  28.5 us
    all_gather x1, waiting for transfers between devices, local(): dy_rows = lax.all_gather(cotangent, 'sp', axis=1, tiled=True)[0]  24 us
    psum x1, blocking collectives, local(): lax.psum((jnp.sum(gate_act, axis=-1), jnp.sum(gate_act * gate_act, axis=-...  13.9 us
    psum x1, blocking collectives, local(): lax.psum(full_bias.astype(jnp.bfloat16), 'sp').astype(jnp.float32)  12 us
    psum x1, blocking collectives, local(): lax.psum(bias_term.astype(jnp.bfloat16), 'dp').astype(jnp.float32)  11.8 us
    psum x1, blocking collectives, local(): lax.psum((jnp.sum(scaled, axis=-1), jnp.sum(scaled * centred, axis=-1)),...  8.36 us
  transfers between devices with their start and end apart: 5, of which 4 were waited for; matrix products, arithmetic and copies ran while one was open for 12% of the time, Pallas kernels for 0%

commit v1 on v0

--- a/solution.py
+++ b/solution.py
@@ -47,7 +47,14 @@
     mixed = (mixed + local_bias.T[None, :, :, None]).reshape(seq_len, channels)
     gated = (unit_act * mixed).astype(jnp.bfloat16)
     weight_whole = lax.all_gather(out_weight, "dp", axis=0, tiled=True)
-    dy_rows = lax.all_gather(cotangent, "sp", axis=1, tiled=True)[0]
+
+    def run_fix(sheet, peer_axis):
+        return jnp.concatenate(
+            lax.all_to_all(jnp.stack(lax.axis_size(peer_axis) * [sheet], axis=0), peer_axis, 0, 0),
+            axis=1,
+        )
+
+    dy_rows = run_fix(cotangent, "sp")[0]
     product = jnp.dot(dy_rows, weight_whole, preferred_element_type=jnp.float32)
     weight_part = lax.dot_general(
         dy_rows, gated, (((0,), (0,)), ((), ())), preferred_element_type=jnp.float32

time: 238 us -> 226 us (0.950)
  waiting for transfers between devices: 136 us -> 93 us
  blocking collectives: 46.1 us -> 68.5 us
  starting transfers between devices: 0.2 us -> 6.64 us
    all_gather x1, waiting for transfers between devices: 28.5 us -> 0.01 us  [local(): weight_whole = lax.all_gather(out_weight, 'dp', axis=0, tiled=True)]
    all_gather x1 -> x0, waiting for transfers between devices: 24 us -> none  [local(): dy_rows = lax.all_gather(cotangent, 'sp', axis=1, tiled=True)[0]]
    psum x1, blocking collectives: 13.9 us -> 36.2 us  [local(): lax.psum((jnp.sum(gate_act, axis=-1), jnp.sum(gate_act * gate_act, axis=-...]
    psum x1, waiting for transfers between devices: 51 us -> 58.9 us  [local(): lax.psum(mix_term.astype(jnp.bfloat16), 'dp').astype(jnp.float32)]
    all_to_all x0 -> x1, starting transfers between devices: none -> 6.48 us  [run_fix(): lax.all_to_all(jnp.stack(lax.axis_size(peer_axis) * [sheet], axis=0), pee...]
    another operation x0 -> x1, local copies, waits for them, and re-layouts: none -> 2.63 us  [run_fix(): jnp.stack(lax.axis_size(peer_axis) * [sheet], axis=0)]
  transfers between devices with their start and end apart: 5 -> 5, of which waited for: 4 -> 3; matrix products, arithmetic and copies ran while one was open for 12% -> 13% of each run, Pallas kernels for 0% -> 0%
where the time goes in v1:
time: 226 us; the launch traced here: 225 us
  waiting for transfers between devices  93 us (41%)
  blocking collectives  68.5 us (30%)
  local copies, waits for them, and re-layouts  17.8 us (8%)
  matrix products  16.3 us (7%)
  between operations  14 us (6%)
  other arithmetic  8.59 us (4%)
  starting transfers between devices  6.64 us (3%)
    psum x1, waiting for transfers between devices, local(): lax.psum(mix_term.astype(jnp.bfloat16), 'dp').astype(jnp.float32)  58.9 us
    psum x1, blocking collectives, local(): lax.psum((jnp.sum(gate_act, axis=-1), jnp.sum(gate_act * gate_act, axis=-...  36.2 us
    reduce_scatter x1, waiting for transfers between devices, local(): lax.psum_scatter(weight_part.astype(jnp.bfloat16), 'dp', scatter_dimensio...  31.6 us
    psum x1, blocking collectives, local(): lax.psum(full_bias.astype(jnp.bfloat16), 'sp').astype(jnp.float32)  12.1 us
    psum x1, blocking collectives, local(): lax.psum(bias_term.astype(jnp.bfloat16), 'dp').astype(jnp.float32)  11.8 us
    psum x1, blocking collectives, local(): lax.psum((jnp.sum(scaled, axis=-1), jnp.sum(scaled * centred, axis=-1)),...  8.36 us
    all_to_all x1, starting transfers between devices, run_fix(): lax.all_to_all(jnp.stack(lax.axis_size(peer_axis) * [sheet], axis=0), pee...  6.48 us
    dot_general x1, matrix products, local(): product = jnp.dot(dy_rows, weight_whole, preferred_element_type=jnp.float32)  5.57 us
  transfers between devices with their start and end apart: 5, of which 3 were waited for; matrix products, arithmetic and copies ran while one was open for 13% of the time, Pallas kernels for 0%

profile of v1, /device:TPU:0, one launch (start us, length us, event | category | flops | bytes accessed | tf_op | source)
XLA Modules:
  0.0 224.9 jit_solution(8193740500244698372)
XLA Ops:
  7.9 2.6 %stack.2 = bf16[4,1,128,2048]{3,2,1,0:T(8,128)(2,1)} broadcast(bf16[128,2048]{1,0:T(8,128)(2,1)} %bitcast.105), dimensions={2,3} | broadcast | bytes 2621440 | tf_op jit(solution)/shard_map/stack | solution.py:53
  10.5 6.5 %all-to-all-start = ((bf16[4,1,128,2048]{3,2,1,0:T(8,128)(2,1)}), bf16[4,1,128,2048]{3,2,1,0:T(8,128)(2,1)}, u32[]{:S(2)}, u32[]{:S(2)}) async-start(bf16[4,1,128,2048]{3,2,1,0:T(8,128)(2,1)} %stack.2), calls=%async_computation | async-start | bytes 4194304 | tf_op jit(solution)/shard_map/all_to_all | solution.py:53
  19.0 1.3 copy.78
  20.8 36.2 %all-reduce.1 = (f32[512]{0:T(512)S(1)}, f32[512]{0:T(512)S(1)}) all-reduce(f32[512]{0:T(512)S(1)} %get-tuple-element.40, f32[512]{0:T(512)S(1)} %get-tuple-element.39), channel_id=1, replica_groups=mesh['sp'=4,'dp'=8] {'sp'}, use_global_device_ids=true, to_apply=%region_3.4 | all-reduce | flops 1024 | bytes 8192 | tf_op jit(solution)/shard_map/psum | solution.py:34
  57.8 3.3 %fusion.40 = (bf16[4,128,2,256]{1,3,0,2:T(8,128)(2,1)}, f32[4,128,2,256]{1,3,0,2:T(8,128)}) fusion(f32[4,128,2,256]{1,3,0,2:T(8,128)} %copy.78, f32[128,2]{0,1:T(2,128)S(1)} %convert_bitcast_fusion.1, bf16[8,128,128]{2,1,0:T(8,128)(2,1)S(1)} %copy-done.7, s32[]{:T(128)S(6)} %select_n.20, pred[128,128]{1,0:T(8,128)(4,1)S(1)} %iota_compare_fusion, ...), kind=kOutput, calls=%fused_computation.61 | convolution fusion | flops 73433088 | bytes 3761156 | tf_op jit(solution)/shard_map/gts,nsgd->ntgd/dot_general | solution.py:46
  61.1 1.5 copy.71
  62.6 1.1 copy.87
  63.7 1.8 all-to-all-done
  65.5 5.6 %fusion.82 = (bf16[512,512]{1,0:T(8,128)(2,1)}, f32[512,512]{1,0:T(8,128)S(1)}, bf16[1,512,512]{2,1,0:T(8,128)(2,1)}) fusion(bf16[1,512,512]{2,1,0:T(8,128)(2,1)S(1)} %copy-done.2, f32[512,512]{1,0:T(8,128)} %bitcast.104, bf16[512,2048]{1,0:T(8,128)(2,1)} %bitcast.1, bf16[2048,512]{1,0:T(8,128)(2,1)} %all-gather.2.cloned.1.call-done), kind=kOutput, calls=%fused_computation.123 | convolution fusion | flops 1081868288 | bytes 7864320 | tf_op jit(solution)/shard_map/dot_general | solution.py:58
  71.1 1.2 reshape.181
  72.3 1.4 fusion.7
  73.7 1.4 copy.79
  76.0 58.9 %all-reduce.6.cloned.1.call-done = bf16[2,128,128]{2,1,0:T(8,128)(2,1)} async-done(((bf16[2,128,128]{2,1,0:T(8,128)(2,1)}), bf16[2,128,128]{2,1,0:T(8,128)(2,1)}) %all-reduce.6.cloned.1.call-update) | async-done | bytes 65552 | tf_op jit(solution)/shard_map/psum | solution.py:96
  136.5 4.3 %fusion = bf16[2048,512]{0,1:T(8,128)(2,1)} fusion(bf16[512,512]{1,0:T(8,128)(2,1)} %bitcast.106, bf16[512,2048]{1,0:T(8,128)(2,1)} %bitcast.1), kind=kOutput, calls=%fused_computation.13 | convolution fusion | flops 1074790400 | bytes 4718592 | tf_op jit(solution)/shard_map/dot_general | solution.py:59
  140.9 1.0 copy-done.4
  141.9 1.8 multiply_reduce_fusion
  144.8 1.6 copy.73
  147.3 11.8 %all-reduce.2 = (bf16[2,128]{1,0:T(2,128)(2,1)S(1)}, bf16[512]{0:T(512)(128)(2,1)S(1)}, bf16[512]{0:T(512)(128)(2,1)S(1)}) all-reduce(bf16[2,128]{1,0:T(2,128)(2,1)S(1)} %bitcast.112, bf16[512]{0:T(512)(128)(2,1)S(1)} %bitcast.110, bf16[512]{0:T(512)(128)(2,1)S(1)} %bitcast.111), channel_id=1, replica_groups=mesh['sp'=4,'dp'=8] {'dp'}, use_global_device_ids=true, to_apply=%region_12.13 | all-reduce | flops 1280 | bytes 5120 | tf_op jit(solution)/shard_map/psum | solution.py:97
  159.2 12.1 %psum.77 = bf16[8,128]{1,0:T(8,128)(2,1)S(1)} all-reduce(bf16[8,128]{1,0:T(8,128)(2,1)S(1)} %dynamic_update_slice.7), channel_id=1, replica_groups=mesh['sp'=4,'dp'=8] {'sp'}, use_global_device_ids=true, to_apply=%region_13.14 | all-reduce | flops 1024 | bytes 4096 | tf_op jit(solution)/shard_map/psum | solution.py:105
  171.3 8.4 %all-reduce = (f32[512]{0:T(512)S(1)}, f32[512]{0:T(512)S(1)}) all-reduce(f32[512]{0:T(512)S(1)} %bitcast.113, f32[512]{0:T(512)S(1)} %bitcast.114), channel_id=1, replica_groups=mesh['sp'=4,'dp'=8] {'sp'}, use_global_device_ids=true, to_apply=%region_7.8 | all-reduce | flops 1024 | bytes 8192 | tf_op jit(solution)/shard_map/psum | solution.py:85
  180.8 2.1 fusion.66
  183.0 1.8 convert_multiply_fusion.9
  184.8 31.6 %reduce-scatter.2.cloned.1.call-done = bf16[256,512]{0,1:T(8,128)(2,1)} async-done(((bf16[2048,512]{0,1:T(8,128)(2,1)}), bf16[256,512]{0,1:T(8,128)(2,1)}) %reduce-scatter.2.cloned.1.call-update) | async-done | bytes 262160 | tf_op jit(solution)/shard_map/reduce_scatter | solution.py:66
  217.3 1.0 copy.83
  (50 shorter events, 10.7 us)
Async XLA Ops:
  7.2 58.4 %all-gather.2.cloned.1.call-start = ((), (), s32[]{:S(2)}) async-start(), calls=%async_computation.2 | async-start | bytes 2359296 | tf_op jit(solution)/shard_map/all_gather | solution.py:49
  10.5 6.6 %copy-start = (bf16[1,512,512]{2,1,0:T(8,128)(2,1)S(1)}, bf16[1,512,512]{2,1,0:T(8,128)(2,1)}, u32[]{:S(2)}) copy-start(bf16[1,512,512]{2,1,0:T(8,128)(2,1)} %param.10) | copy-start | bytes 1572868
  10.5 55.0 %all-to-all-start = ((bf16[4,1,128,2048]{3,2,1,0:T(8,128)(2,1)}), bf16[4,1,128,2048]{3,2,1,0:T(8,128)(2,1)}, u32[]{:S(2)}, u32[]{:S(2)}) async-start(bf16[4,1,128,2048]{3,2,1,0:T(8,128)(2,1)} %stack.2), calls=%async_computation | async-start | bytes 4194304 | tf_op jit(solution)/shard_map/all_to_all | solution.py:53
  17.0 1.3 copy-start.5
  17.0 1.3 copy-start.6
  17.0 1.3 copy-start.2
  17.0 117.8 %all-reduce.6.cloned.1.call-start = ((), (), s32[]{:S(2)}) async-start(), calls=%async_computation.4 | async-start | bytes 131072 | tf_op jit(solution)/shard_map/psum | solution.py:96
  18.3 39.5 %copy-start.7 = (bf16[8,128,128]{2,1,0:T(8,128)(2,1)S(1)}, bf16[8,128,128]{2,1,0:T(8,128)(2,1)}, u32[]{:S(2)}) copy-start(bf16[8,128,128]{2,1,0:T(8,128)(2,1)} %param.12) | copy-start | bytes 786436
  72.3 1.4 copy-start.3
  73.7 109.3 %all-reduce.8.cloned.1.call-start = ((), (), s32[]{:S(2)}) async-start(), calls=%async_computation.5 | async-start | bytes 524288 | tf_op jit(solution)/shard_map/psum | solution.py:104
  135.8 0.7 copy-start.1
  136.5 79.9 %reduce-scatter.2.cloned.1.call-start = ((), (), s32[]{:S(2)}) async-start(), calls=%async_computation.3 | async-start | bytes 2359296 | tf_op jit(solution)/shard_map/reduce_scatter | solution.py:66
  140.9 1.0 copy-start.4
Sparse Core Ops, SparseCore 0:
  9.9 30.4 all-gather.1
  73.8 61.0 all-reduce.5
  137.2 34.9 all-reduce.7
  175.4 40.9 reduce-scatter.1
